TPU v7x, 32 devices: a whole 2x2x4 slice. The times are simulated.
32 devices in a mesh: ep: 8 (over z, x), tp: 4 (over y, core).
Axes of the slice: x: 2, y: 2, z: 4, core: 2. Of those that a mesh axis runs over, the one named last changes fastest.
Arguments:
- query_rows: bfloat16 [3072, 1024], P('ep', 'tp'), may hold values from -8 to 8
- key_rows: bfloat16 [3072, 256], P('ep'), may hold values from -8 to 8
- value_rows: bfloat16 [3072, 256], P('ep'), may hold values from -6 to 6
- query_gain: float32 [64], replicated, may hold values from 0.3 to 6
- key_gain: float32 [64], replicated, may hold values from 0.3 to 6
- out_weight: bfloat16 [1024, 2048], P('tp'), may hold values from -0.1875 to 0.1875
- mixer_gain: float32 [2048], replicated, may hold values from 0.1 to 1.9
- expert_input: bfloat16 [2048, 2048], P('ep'), may hold values from -6 to 6
- expert_ids: int32 [2048, 2], P('ep'), may hold values from 0 to 7, all different within a row; in each aligned block of 256 rows (0 to 255, 256 to 511, ...) at most 96 rows name the same one
- gate_score: float32 [2048, 2], P('ep'), may hold values from 0.05 to 1
- expert_gain: float32 [2048], replicated, may hold values from 0.1 to 1.9
- gate_weight: bfloat16 [8, 2048, 4096], P('ep', None, 'tp'), may hold values from -0.125 to 0.125
- up_weight: bfloat16 [8, 2048, 4096], P('ep', None, 'tp'), may hold values from -0.125 to 0.125
- down_weight: bfloat16 [8, 4096, 2048], P('ep', 'tp'), may hold values from -0.09375 to 0.09375
- shared_gate: bfloat16 [2048, 2048], P(None, 'tp'), may hold values from -0.125 to 0.125
- shared_up: bfloat16 [2048, 2048], P(None, 'tp'), may hold values from -0.125 to 0.125
- shared_down: bfloat16 [2048, 2048], P('tp'), may hold values from -0.125 to 0.125
Outputs:
- mixer_out: bfloat16 [3072, 2048], P('ep')
- expert_out: bfloat16 [2048, 2048], P('ep', 'tp')
Inputs may be any that keep to these rules, and one draw needn't show every extreme that they name: `expert_ids`: each row names 2 different experts. In each aligned block of 256 rows (the rows of one device) no expert is named by more than 96 rows, a bound that some block reaches.
All inputs are finite; a program needn't handle non-finite values.
Results may differ from a plain program's by a relative error of at most 0.02.
The roundings to bfloat16 on the way count: a program that leaves them out, or rounds other values in their place, can miss the bound.
Values may be sent and summed in bfloat16 or wider, within the bound.
A program may use at most 128 MiB of HBM per device.

v0:
```python
import math

import jax
import jax.numpy as jnp
from jax import lax
from jax.sharding import PartitionSpec as P

HEADS = 16
KV_HEADS = 4
HEAD_DIM = 64
GRID_W = 64


EPSILON = 1e-06
ROUTED_SCALE = 2.5


def rotary_angles(position):
    grid_row = (position // GRID_W).astype(jnp.float32)
    grid_col = (position % GRID_W).astype(jnp.float32)
    quarter = HEAD_DIM // 4
    inverse = 10000.0 ** (-jnp.arange(quarter, dtype=jnp.float32) / quarter)
    return jnp.concatenate([grid_row[:, None] * inverse, grid_col[:, None] * inverse], axis=1)


def normalize_rotate(heads_in, gain_vector, angles):
    widened = heads_in.astype(jnp.float32)
    scaled = widened * lax.rsqrt(jnp.mean(widened * widened, axis=-1, keepdims=True) + EPSILON)
    scaled = scaled * gain_vector
    half_dim = scaled.shape[-1] // 2
    front_half = scaled[..., :half_dim]
    back_half = scaled[..., half_dim:]
    cosine_table = jnp.cos(angles)[:, None, :]
    sine_table = jnp.sin(angles)[:, None, :]
    turned = jnp.concatenate(
        [
            front_half * cosine_table - back_half * sine_table,
            front_half * sine_table + back_half * cosine_table,
        ],
        axis=-1,
    )
    return turned.astype(jnp.bfloat16)


def mixer_half(query_rows, key_rows, value_rows, query_gain, key_gain, out_weight, mixer_gain):
    local_rows = query_rows.shape[0]
    lane_heads = query_rows.shape[1] // HEAD_DIM
    group = HEADS // KV_HEADS
    lane_kv = max(1, lane_heads // group)
    local_group = lane_heads // lane_kv
    first_kv = lax.axis_index("tp") * lane_heads // group
    offset = lax.axis_index("ep") * local_rows
    angles = rotary_angles(offset + jnp.arange(local_rows, dtype=jnp.int32))
    query_rot = normalize_rotate(
        query_rows.reshape(local_rows, lane_heads, HEAD_DIM), query_gain, angles
    )
    query_grouped = query_rot.reshape(local_rows, lane_kv, local_group, HEAD_DIM)
    key_cols = lax.dynamic_slice_in_dim(key_rows, first_kv * HEAD_DIM, lane_kv * HEAD_DIM, 1)
    value_cols = lax.dynamic_slice_in_dim(value_rows, first_kv * HEAD_DIM, lane_kv * HEAD_DIM, 1)
    key_rot = normalize_rotate(key_cols.reshape(local_rows, lane_kv, HEAD_DIM), key_gain, angles)
    stacked = jnp.concatenate([key_rot.reshape(local_rows, lane_kv * HEAD_DIM), value_cols], axis=1)
    scale_factor = HEAD_DIM ** (-0.5)
    key_width = lane_kv * HEAD_DIM

    def step_block(state, block_rows):
        row_peak, row_total, accum = state
        block_keys = block_rows[:, :key_width].reshape(block_rows.shape[0], lane_kv, HEAD_DIM)
        block_values = block_rows[:, key_width:].reshape(block_rows.shape[0], lane_kv, HEAD_DIM)
        scores = (
            jnp.einsum(
                "qkgd,skd->kgqs", query_grouped, block_keys, preferred_element_type=jnp.float32
            )
            * scale_factor
        )
        new_peak = jnp.maximum(row_peak, jnp.max(scores, axis=3))
        shrink = jnp.exp(row_peak - new_peak)
        exponent = jnp.exp(scores - new_peak[..., None])
        row_total = row_total * shrink + jnp.sum(exponent, axis=3)
        accum = accum * shrink[..., None] + jnp.einsum(
            "kgqs,skd->kgqd",
            exponent.astype(jnp.bfloat16),
            block_values,
            preferred_element_type=jnp.float32,
        )
        return ((new_peak, row_total, accum), None)

    start_state = (
        jnp.full((lane_kv, local_group, local_rows), -jnp.inf, jnp.float32),
        jnp.zeros((lane_kv, local_group, local_rows), jnp.float32),
        jnp.zeros((lane_kv, local_group, local_rows, HEAD_DIM), jnp.float32),
    )
    carry = start_state
    piece = lax.all_gather(stacked, "ep", axis=0, tiled=True)
    shard_count = piece.shape[0] // local_rows
    per_block = math.gcd(shard_count, max(1, 2048 // local_rows))
    block_rows = per_block * local_rows
    blocks = piece.reshape(piece.shape[0] // block_rows, block_rows, piece.shape[1])
    carry, unused = lax.scan(step_block, carry, blocks)
    row_peak, row_total, accum = carry
    attended = (accum / row_total[..., None]).astype(jnp.bfloat16)
    lane_weight = out_weight.reshape(lane_kv, local_group, HEAD_DIM, out_weight.shape[1])
    partial_value = jnp.einsum(
        "kgqd,kgde->qe", attended, lane_weight, preferred_element_type=jnp.float32
    )
    mixer_sum = lax.psum(partial_value.astype(jnp.bfloat16), "tp").astype(jnp.float32)
    mixer_scale = lax.rsqrt(jnp.mean(mixer_sum * mixer_sum, axis=1, keepdims=True) + EPSILON)
    return (mixer_sum * mixer_scale * mixer_gain).astype(jnp.bfloat16)


def expert_half(
    expert_input,
    expert_ids,
    gate_score,
    expert_gain,
    gate_weight,
    up_weight,
    down_weight,
    shared_gate,
    shared_up,
    shared_down,
):
    local_rows, top_count = expert_ids.shape
    local_experts = gate_weight.shape[0]
    ep_size = lax.axis_size("ep")
    experts_all = local_experts * ep_size
    capacity = 3 * local_rows * top_count // (2 * experts_all)
    model_width = expert_input.shape[1]
    lane_cols = model_width // lax.axis_size("tp")
    slots_total = ep_size * capacity
    widened = expert_input.astype(jnp.float32)
    normed = (
        widened
        * lax.rsqrt(jnp.mean(widened * widened, axis=1, keepdims=True) + EPSILON)
        * expert_gain
    ).astype(jnp.bfloat16)
    route_weight = gate_score / jnp.sum(gate_score, axis=1, keepdims=True) * ROUTED_SCALE
    pair_ids = expert_ids.reshape(local_rows * top_count)
    onehot = (pair_ids[:, None] == jnp.arange(experts_all, dtype=jnp.int32)).astype(jnp.int32)
    ranks = jnp.sum(
        (jnp.cumsum(onehot, axis=0, dtype=jnp.int32) - 1) * onehot, axis=1, dtype=jnp.int32
    )
    slot_index = pair_ids * capacity + ranks
    row_numbers = jnp.arange(local_rows * top_count, dtype=jnp.int32) // top_count
    sources = jnp.full((experts_all * capacity,), -1, jnp.int32).at[slot_index].set(row_numbers)
    filled = (sources >= 0)[:, None]
    safe_rows = jnp.maximum(sources, 0)
    nothing = jnp.zeros((), jnp.bfloat16)
    lane_start = lax.axis_index("tp") * lane_cols
    own_cols = lax.dynamic_slice_in_dim(normed, lane_start, lane_cols, 1)
    outgoing = jnp.where(filled, own_cols[safe_rows], nothing).reshape(
        experts_all, capacity, lane_cols
    )
    arrived = lax.all_to_all(outgoing, "ep", split_axis=0, concat_axis=0, tiled=True)
    arranged = arrived.reshape(ep_size, local_experts, capacity, lane_cols).transpose(1, 0, 2, 3)
    arranged = arranged.reshape(local_experts, slots_total, lane_cols)
    piece = lax.all_gather(arranged, "tp", axis=2, tiled=True)
    gate_value = jnp.einsum("esd,edf->esf", piece, gate_weight, preferred_element_type=jnp.float32)
    up_value = jnp.einsum("esd,edf->esf", piece, up_weight, preferred_element_type=jnp.float32)
    hidden = (jax.nn.silu(gate_value) * up_value).astype(jnp.bfloat16)
    down_part = jnp.einsum("esf,efd->esd", hidden, down_weight, preferred_element_type=jnp.float32)
    down_rows = down_part.reshape(local_experts, ep_size, capacity, model_width).transpose(
        1, 0, 2, 3
    )
    down_rows = down_rows.reshape(experts_all * capacity, model_width)
    shared_gate_value = jnp.dot(normed, shared_gate, preferred_element_type=jnp.float32)
    shared_up_value = jnp.dot(normed, shared_up, preferred_element_type=jnp.float32)
    shared_hidden = (jax.nn.silu(shared_gate_value) * shared_up_value).astype(jnp.bfloat16)
    shared_part = jnp.dot(shared_hidden, shared_down, preferred_element_type=jnp.float32)
    terms = jnp.concatenate([down_rows, shared_part], axis=0)
    summed = lax.psum_scatter(
        terms.astype(jnp.bfloat16), "tp", scatter_dimension=1, tiled=True
    ).astype(jnp.float32)
    routed_slots = (
        summed[: experts_all * capacity]
        .astype(jnp.bfloat16)
        .reshape(experts_all, capacity, lane_cols)
    )
    shared_cols = summed[experts_all * capacity :]
    returned = lax.all_to_all(routed_slots, "ep", split_axis=0, concat_axis=0, tiled=True)
    picked = returned.reshape(experts_all * capacity, lane_cols)[slot_index]
    picked = picked.reshape(local_rows, top_count, lane_cols)
    routed = jnp.sum(picked.astype(jnp.float32) * route_weight[:, :, None], axis=1)
    return (routed + shared_cols).astype(jnp.bfloat16)


def body(
    query_rows,
    key_rows,
    value_rows,
    query_gain,
    key_gain,
    out_weight,
    mixer_gain,
    expert_input,
    expert_ids,
    gate_score,
    expert_gain,
    gate_weight,
    up_weight,
    down_weight,
    shared_gate,
    shared_up,
    shared_down,
):
    mixer_out = mixer_half(
        query_rows, key_rows, value_rows, query_gain, key_gain, out_weight, mixer_gain
    )
    expert_out = expert_half(
        expert_input,
        expert_ids,
        gate_score,
        expert_gain,
        gate_weight,
        up_weight,
        down_weight,
        shared_gate,
        shared_up,
        shared_down,
    )
    return (mixer_out, expert_out)


def solution(mesh):
    in_specs = (
        P("ep", "tp"),
        P("ep", None),
        P("ep", None),
        P(),
        P(),
        P("tp", None),
        P(),
        P("ep", None),
        P("ep", None),
        P("ep", None),
        P(),
        P("ep", None, "tp"),
        P("ep", None, "tp"),
        P("ep", "tp", None),
        P(None, "tp"),
        P(None, "tp"),
        P("tp", None),
    )
    out_specs = (P("ep", None), P("ep", "tp"))
    return jax.shard_map(body, mesh=mesh, in_specs=in_specs, out_specs=out_specs, check_vma=False)
```

profile of v0, /device:TPU:27, one launch (start us, length us, event | category | flops | bytes accessed | tf_op | source)
XLA Modules:
  0.0 216.5 jit_solution(9273533455983463291)
XLA Ops:
  11.0 2.4 %scatter_custom_fusion = s32[768]{0:T(1024)S(1)} fusion(s32[512]{0:T(512)S(1)} %bitcast.141, s32[512]{0:T(512)S(1)} %add_select_fusion, s32[]{:T(128)} %constant.116.clone.1), kind=kCustom, calls=%fused_computation.114 | custom fusion | bytes 3076 | tf_op jit(solution)/shard_map/scatter | solution.py:144
  17.1 2.7 %gather_fusion = bf16[768,512]{1,0:T(8,128)(2,1)S(1)} fusion(bf16[256,512]{1,0:T(8,128)(2,1)S(1)} %constant_dynamic-slice_fusion.1, s32[1024]{0:T(1024)S(1)} %pad_clamp_fusion.1), kind=kCustom, calls=%fused_computation | custom fusion | bytes 1575936 | tf_op jit(solution)/shard_map/gather | solution.py:150
  20.0 23.3 %all_to_all.10 = bf16[8,96,512]{2,1,0:T(8,128)(2,1)} all-to-all(bf16[8,96,512]{2,1,0:T(8,128)(2,1)S(1)} %broadcast_select_fusion), channel_id=1, replica_groups=mesh['ep'=8,'tp'=4] {'ep'}, dimensions={0} | all-to-all | bytes 1572864 | tf_op jit(solution)/shard_map/all_to_all | solution.py:153
  46.7 3.1 %fusion.67 = f32[256,512]{1,0:T(8,128)} fusion(bf16[256,2048]{1,0:T(8,128)(2,1)S(1)} %copy-done.5, bf16[2048,512]{1,0:T(8,128)(2,1)} %param.33), kind=kOutput, calls=%fused_computation.131 | convolution fusion | flops 536870912 | bytes 3670016 | tf_op jit(solution)/shard_map/dot_general | solution.py:165
  49.8 29.0 %all_gather.6 = bf16[3072,128]{1,0:T(8,128)(2,1)} all-gather(bf16[384,128]{1,0:T(8,128)(2,1)S(1)} %pad_maximum_fusion.2), channel_id=1, replica_groups=mesh['ep'=8,'tp'=4] {'ep'}, dimensions={0}, use_global_device_ids=true | all-gather | bytes 884736 | tf_op jit(solution)/shard_map/all_gather | solution.py:93
  78.8 4.3 %convolution_convert_fusion = bf16[256,2048]{1,0:T(8,128)(2,1)} fusion(bf16[512,2048]{1,0:T(8,128)(2,1)S(1)} %copy-done, bf16[256,2048]{1,0:T(8,128)(2,1)} %copy-done.4, bf16[2048,512]{1,0:T(8,128)(2,1)} %param.34, f32[256,512]{1,0:T(8,128)} %fusion.67), kind=kOutput, calls=%fused_computation.44 | convolution fusion | flops 1075052544 | bytes 6815744 | tf_op jit(solution)/shard_map/dot_general | solution.py:168
  83.1 6.3 %fusion.16 = f32[768,1024]{1,0:T(8,128)S(1)} fusion(bf16[1,2048,1024]{2,1,0:T(8,128)(2,1)} %param.30, bf16[1,768,2048]{2,1,0:T(8,128)(2,1)} %all-gather.2.cloned.1.call-done), kind=kOutput, calls=%fused_computation.30 | convolution fusion | flops 3221225472 | bytes 10485760 | tf_op jit(solution)/shard_map/esd,edf->esf/dot_general | solution.py:157
  89.4 3.6 %multiply_convert_fusion = bf16[768,1024]{1,0:T(8,128)(2,1)S(1)} fusion(f32[768,1024]{1,0:T(8,128)S(1)} %fusion.16, bf16[1,2048,1024]{2,1,0:T(8,128)(2,1)S(1)} %copy-done.12, bf16[1,768,2048]{2,1,0:T(8,128)(2,1)S(1)} %copy-done.14), kind=kOutput, calls=%fused_computation.41 | convolution fusion | flops 3225944064 | bytes 12058624 | tf_op jit(solution)/shard_map/esd,edf->esf/dot_general | solution.py:158
  93.1 3.6 %fusion.18 = bf16[768,2048]{1,0:T(8,128)(2,1)S(1)} fusion(bf16[768,1024]{1,0:T(8,128)(2,1)S(1)} %multiply_convert_fusion, bf16[1,1024,2048]{2,1,0:T(8,128)(2,1)S(1)} %copy-done.13), kind=kOutput, calls=%fused_computation.34 | convolution fusion | flops 3222798336 | bytes 8912896 | tf_op jit(solution)/shard_map/esf,efd->esd/dot_general | solution.py:160
  96.7 2.2 %pad_maximum_fusion = bf16[1024,2048]{1,0:T(8,128)(2,1)} fusion(bf16[256,2048]{1,0:T(8,128)(2,1)S(1)} %copy-done.6, bf16[768,2048]{1,0:T(8,128)(2,1)S(1)} %fusion.18), kind=kLoop, calls=%fused_computation.25 | loop fusion | flops 8388608 | bytes 8388608 | tf_op jit(solution)/shard_map/concatenate | solution.py:169
  99.0 47.7 %while.15 = (s32[]{:T(128)}, f32[1,4,384]{2,1,0:T(4,128)S(1)}, f32[1,4,384]{2,1,0:T(4,128)S(1)}, f32[1,4,384,64]{2,3,1,0:T(8,128)S(1)}, bf16[8,384,128]{2,1,0:T(...) while((s32[]{:T(128)}, f32[1,4,384]{2,1,0:T(4,128)S(1)}, ...), condition=%wide.region_5.6_spmd.clone, body=%wide.region_2.5_spmd.clone.sunk | while | flops 156017664 | bytes 18088064 | solution.py:98
  102.0 2.4 %fusion.82 = f32[1,4,384,64]{2,3,1,0:T(8,128)S(1)} fusion(f32[384,384,4]{1,0,2:T(8,128)} %get-tuple-element.151, f32[4,384]{1,0:T(4,128)S(1)} %bitcast.134, f32[1,4,384,64]{2,3,1,0:T(8,128)S(1)} %get-tuple-element.164, f32[4,384]{1,0:T(4,128)S(1)} %get-tuple-element.152, pred[]{:T(512)S(6)} %compare.18, bf16[384,128]{0,1:T(8,128)(2,1)S(1)} %bitcast.133), kind=kOutput, calls=%fused_computation.9.clone.1 | convolution fusion | flops 77561856 | bytes 3207169 | tf_op jit(solution)/shard_map/while/body/eval_jaxpr/kgqs,skd->kgqd/dot_general | solution.py:79
  107.8 2.4 %fusion.82 = f32[1,4,384,64]{2,3,1,0:T(8,128)S(1)} fusion(f32[384,384,4]{1,0,2:T(8,128)} %get-tuple-element.151, f32[4,384]{1,0:T(4,128)S(1)} %bitcast.134, f32[1,4,384,64]{2,3,1,0:T(8,128)S(1)} %get-tuple-element.164, f32[4,384]{1,0:T(4,128)S(1)} %get-tuple-element.152, pred[]{:T(512)S(6)} %compare.18, bf16[384,128]{0,1:T(8,128)(2,1)S(1)} %bitcast.133), kind=kOutput, calls=%fused_computation.9.clone.1 | convolution fusion | flops 77561856 | bytes 3207169 | tf_op jit(solution)/shard_map/while/body/eval_jaxpr/kgqs,skd->kgqd/dot_general | solution.py:79
  113.7 3.1 %fusion.82 = f32[1,4,384,64]{2,3,1,0:T(8,128)S(1)} fusion(f32[384,384,4]{1,0,2:T(8,128)} %get-tuple-element.151, f32[4,384]{1,0:T(4,128)S(1)} %bitcast.134, f32[1,4,384,64]{2,3,1,0:T(8,128)S(1)} %get-tuple-element.164, f32[4,384]{1,0:T(4,128)S(1)} %get-tuple-element.152, pred[]{:T(512)S(6)} %compare.18, bf16[384,128]{0,1:T(8,128)(2,1)S(1)} %bitcast.133), kind=kOutput, calls=%fused_computation.9.clone.1 | convolution fusion | flops 77561856 | bytes 3207169 | tf_op jit(solution)/shard_map/while/body/eval_jaxpr/kgqs,skd->kgqd/dot_general | solution.py:79
  120.4 2.4 %fusion.82 = f32[1,4,384,64]{2,3,1,0:T(8,128)S(1)} fusion(f32[384,384,4]{1,0,2:T(8,128)} %get-tuple-element.151, f32[4,384]{1,0:T(4,128)S(1)} %bitcast.134, f32[1,4,384,64]{2,3,1,0:T(8,128)S(1)} %get-tuple-element.164, f32[4,384]{1,0:T(4,128)S(1)} %get-tuple-element.152, pred[]{:T(512)S(6)} %compare.18, bf16[384,128]{0,1:T(8,128)(2,1)S(1)} %bitcast.133), kind=kOutput, calls=%fused_computation.9.clone.1 | convolution fusion | flops 77561856 | bytes 3207169 | tf_op jit(solution)/shard_map/while/body/eval_jaxpr/kgqs,skd->kgqd/dot_general | solution.py:79
  126.2 2.4 %fusion.82 = f32[1,4,384,64]{2,3,1,0:T(8,128)S(1)} fusion(f32[384,384,4]{1,0,2:T(8,128)} %get-tuple-element.151, f32[4,384]{1,0:T(4,128)S(1)} %bitcast.134, f32[1,4,384,64]{2,3,1,0:T(8,128)S(1)} %get-tuple-element.164, f32[4,384]{1,0:T(4,128)S(1)} %get-tuple-element.152, pred[]{:T(512)S(6)} %compare.18, bf16[384,128]{0,1:T(8,128)(2,1)S(1)} %bitcast.133), kind=kOutput, calls=%fused_computation.9.clone.1 | convolution fusion | flops 77561856 | bytes 3207169 | tf_op jit(solution)/shard_map/while/body/eval_jaxpr/kgqs,skd->kgqd/dot_general | solution.py:79
  132.0 2.5 %fusion.82 = f32[1,4,384,64]{2,3,1,0:T(8,128)S(1)} fusion(f32[384,384,4]{1,0,2:T(8,128)} %get-tuple-element.151, f32[4,384]{1,0:T(4,128)S(1)} %bitcast.134, f32[1,4,384,64]{2,3,1,0:T(8,128)S(1)} %get-tuple-element.164, f32[4,384]{1,0:T(4,128)S(1)} %get-tuple-element.152, pred[]{:T(512)S(6)} %compare.18, bf16[384,128]{0,1:T(8,128)(2,1)S(1)} %bitcast.133), kind=kOutput, calls=%fused_computation.9.clone.1 | convolution fusion | flops 77561856 | bytes 3207169 | tf_op jit(solution)/shard_map/while/body/eval_jaxpr/kgqs,skd->kgqd/dot_general | solution.py:79
  137.9 2.4 %fusion.82 = f32[1,4,384,64]{2,3,1,0:T(8,128)S(1)} fusion(f32[384,384,4]{1,0,2:T(8,128)} %get-tuple-element.151, f32[4,384]{1,0:T(4,128)S(1)} %bitcast.134, f32[1,4,384,64]{2,3,1,0:T(8,128)S(1)} %get-tuple-element.164, f32[4,384]{1,0:T(4,128)S(1)} %get-tuple-element.152, pred[]{:T(512)S(6)} %compare.18, bf16[384,128]{0,1:T(8,128)(2,1)S(1)} %bitcast.133), kind=kOutput, calls=%fused_computation.9.clone.1 | convolution fusion | flops 77561856 | bytes 3207169 | tf_op jit(solution)/shard_map/while/body/eval_jaxpr/kgqs,skd->kgqd/dot_general | solution.py:79
  143.8 2.4 %fusion.82 = f32[1,4,384,64]{2,3,1,0:T(8,128)S(1)} fusion(f32[384,384,4]{1,0,2:T(8,128)} %get-tuple-element.151, f32[4,384]{1,0:T(4,128)S(1)} %bitcast.134, f32[1,4,384,64]{2,3,1,0:T(8,128)S(1)} %get-tuple-element.164, f32[4,384]{1,0:T(4,128)S(1)} %get-tuple-element.152, pred[]{:T(512)S(6)} %compare.18, bf16[384,128]{0,1:T(8,128)(2,1)S(1)} %bitcast.133), kind=kOutput, calls=%fused_computation.9.clone.1 | convolution fusion | flops 77561856 | bytes 3207169 | tf_op jit(solution)/shard_map/while/body/eval_jaxpr/kgqs,skd->kgqd/dot_general | solution.py:79
  146.7 3.0 %bitcast_convert_fusion = bf16[384,2048]{1,0:T(8,128)(2,1)} fusion(bf16[4,64,2048]{2,1,0:T(8,128)(2,1)} %bitcast.144, f32[1,4,384,64]{2,3,1,0:T(8,128)S(1)} %get-tuple-element.35, f32[4,384]{1,0:T(4,128)S(1)} %bitcast.140), kind=kOutput, calls=%fused_computation.40 | convolution fusion | flops 403636224 | bytes 3020800 | tf_op jit(solution)/shard_map/kgqd,kgde->qe/dot_general | solution.py:102
  149.9 2.1 slice.56
  152.0 5.4 %all-to-all-start.1 = ((bf16[8,96,512]{2,1,0:T(8,128)(2,1)}), bf16[8,96,512]{2,1,0:T(8,128)(2,1)S(1)}, u32[]{:S(2)}, u32[]{:S(2)}) async-start(bf16[8,96,512]{2,1,0:T(8,128)(2,1)} %bitcast.137), calls=%async_computation.2 | async-start | bytes 1572864 | tf_op jit(solution)/shard_map/all_to_all | solution.py:179
  157.6 41.4 %all-reduce.2.cloned.1.call-done = bf16[384,2048]{1,0:T(8,128)(2,1)} async-done(((bf16[384,2048]{1,0:T(8,128)(2,1)}), bf16[384,2048]{1,0:T(8,128)(2,1)}) %all-reduce.2.cloned.1.call-update) | async-done | bytes 1572880 | tf_op jit(solution)/shard_map/psum | solution.py:105
  202.6 2.6 %gather_fusion.1 = bf16[512,512]{1,0:T(8,128)(2,1)} fusion(bf16[768,512]{1,0:T(8,128)(2,1)S(1)} %bitcast.131, s32[1024]{0:T(1024)S(1)} %pad_clamp_fusion), kind=kCustom, calls=%fused_computation.1 | custom fusion | bytes 1050624 | tf_op jit(solution)/shard_map/gather | solution.py:180
  (164 shorter events, 46.8 us)
Async XLA Ops:
  7.2 71.6 %copy-start = (bf16[512,2048]{1,0:T(8,128)(2,1)S(1)}, bf16[512,2048]{1,0:T(8,128)(2,1)}, u32[]{:S(2)}) copy-start(bf16[512,2048]{1,0:T(8,128)(2,1)} %param.35) | copy-start | bytes 6291460
  7.2 8.0 %copy-start.3 = (bf16[256,2048]{1,0:T(8,128)(2,1)S(1)}, bf16[256,2048]{1,0:T(8,128)(2,1)}, u32[]{:S(2)}) copy-start(bf16[256,2048]{1,0:T(8,128)(2,1)} %param.26) | copy-start | bytes 3145732
  7.2 75.9 %all-gather.2.cloned.1.call-start = ((), (), s32[]{:S(2)}) async-start(), calls=%async_computation.4 | async-start | bytes 3932160 | tf_op jit(solution)/shard_map/all_gather | solution.py:156
  19.8 25.0 %copy-start.10 = (f32[64]{0:T(128)S(1)}, f32[64]{0:T(128)}, u32[]{:S(2)}) copy-start(f32[64]{0:T(128)} %param.23) | copy-start | bytes 772
  19.8 25.5 %copy-start.7 = (bf16[384,256]{1,0:T(8,128)(2,1)S(1)}, bf16[384,256]{1,0:T(8,128)(2,1)}, u32[]{:S(2)}) copy-start(bf16[384,256]{1,0:T(8,128)(2,1)} %param.19) | copy-start | bytes 589828
  20.0 25.9 %copy-start.11 = (f32[64]{0:T(128)S(1)}, f32[64]{0:T(128)}, u32[]{:S(2)}) copy-start(f32[64]{0:T(128)} %param.22) | copy-start | bytes 772
  43.4 106.5 %reduce-scatter.2.cloned.1.call-start = ((), (), s32[]{:S(2)}) async-start(), calls=%async_computation.5 | async-start | bytes 5242880 | tf_op jit(solution)/shard_map/reduce_scatter | solution.py:170
  83.1 6.3 %copy-start.12 = (bf16[1,2048,1024]{2,1,0:T(8,128)(2,1)S(1)}, bf16[1,2048,1024]{2,1,0:T(8,128)(2,1)}, u32[]{:S(2)}) copy-start(bf16[1,2048,1024]{2,1,0:T(8,128)(2,1)} %param.31) | copy-start | bytes 12582916
  83.1 6.3 %copy-start.14 = (bf16[1,768,2048]{2,1,0:T(8,128)(2,1)S(1)}, bf16[1,768,2048]{2,1,0:T(8,128)(2,1)}, u32[]{:S(2)}) copy-start(bf16[1,768,2048]{2,1,0:T(8,128)(2,1)} %all-gather.2.cloned.1.call-done) | copy-start | bytes 9437188
  89.4 3.6 %copy-start.13 = (bf16[1,1024,2048]{2,1,0:T(8,128)(2,1)S(1)}, bf16[1,1024,2048]{2,1,0:T(8,128)(2,1)}, u32[]{:S(2)}) copy-start(bf16[1,1024,2048]{2,1,0:T(8,128)(2,1)} %param.32) | copy-start | bytes 12582916
  93.1 3.6 %copy-start.6 = (bf16[256,2048]{1,0:T(8,128)(2,1)S(1)}, bf16[256,2048]{1,0:T(8,128)(2,1)}, u32[]{:S(2)}) copy-start(bf16[256,2048]{1,0:T(8,128)(2,1)} %convolution_convert_fusion) | copy-start | bytes 3145732
  99.0 100.1 %all-reduce.2.cloned.1.call-start = ((), (), s32[]{:S(2)}) async-start(), calls=%async_computation.3 | async-start | bytes 3145728 | tf_op jit(solution)/shard_map/psum | solution.py:105
  102.0 2.4 %copy-start.1 = (f32[384,384,4]{1,0,2:T(8,128)S(1)}, f32[384,384,4]{1,0,2:T(8,128)}, u32[]{:S(2)}) copy-start(f32[384,384,4]{1,0,2:T(8,128)} %get-tuple-element.151) | copy-start | bytes 7077892 | tf_op jit(solution)/shard_map/while
  107.8 2.4 %copy-start.1 = (f32[384,384,4]{1,0,2:T(8,128)S(1)}, f32[384,384,4]{1,0,2:T(8,128)}, u32[]{:S(2)}) copy-start(f32[384,384,4]{1,0,2:T(8,128)} %get-tuple-element.151) | copy-start | bytes 7077892 | tf_op jit(solution)/shard_map/while
  113.7 3.3 %copy-start.1 = (f32[384,384,4]{1,0,2:T(8,128)S(1)}, f32[384,384,4]{1,0,2:T(8,128)}, u32[]{:S(2)}) copy-start(f32[384,384,4]{1,0,2:T(8,128)} %get-tuple-element.151) | copy-start | bytes 7077892 | tf_op jit(solution)/shard_map/while
  120.4 2.4 %copy-start.1 = (f32[384,384,4]{1,0,2:T(8,128)S(1)}, f32[384,384,4]{1,0,2:T(8,128)}, u32[]{:S(2)}) copy-start(f32[384,384,4]{1,0,2:T(8,128)} %get-tuple-element.151) | copy-start | bytes 7077892 | tf_op jit(solution)/shard_map/while
  126.2 2.4 %copy-start.1 = (f32[384,384,4]{1,0,2:T(8,128)S(1)}, f32[384,384,4]{1,0,2:T(8,128)}, u32[]{:S(2)}) copy-start(f32[384,384,4]{1,0,2:T(8,128)} %get-tuple-element.151) | copy-start | bytes 7077892 | tf_op jit(solution)/shard_map/while
  132.0 2.5 %copy-start.1 = (f32[384,384,4]{1,0,2:T(8,128)S(1)}, f32[384,384,4]{1,0,2:T(8,128)}, u32[]{:S(2)}) copy-start(f32[384,384,4]{1,0,2:T(8,128)} %get-tuple-element.151) | copy-start | bytes 7077892 | tf_op jit(solution)/shard_map/while
  137.9 2.5 %copy-start.1 = (f32[384,384,4]{1,0,2:T(8,128)S(1)}, f32[384,384,4]{1,0,2:T(8,128)}, u32[]{:S(2)}) copy-start(f32[384,384,4]{1,0,2:T(8,128)} %get-tuple-element.151) | copy-start | bytes 7077892 | tf_op jit(solution)/shard_map/while
  143.8 2.4 %copy-start.1 = (f32[384,384,4]{1,0,2:T(8,128)S(1)}, f32[384,384,4]{1,0,2:T(8,128)}, u32[]{:S(2)}) copy-start(f32[384,384,4]{1,0,2:T(8,128)} %get-tuple-element.151) | copy-start | bytes 7077892 | tf_op jit(solution)/shard_map/while
  149.7 7.7 %copy-start.9 = (f32[256,2]{0,1:T(2,128)S(1)}, f32[256,2]{0,1:T(2,128)}, u32[]{:S(2)}) copy-start(f32[256,2]{0,1:T(2,128)} %param.28) | copy-start | bytes 6148
  149.7 51.3 %copy-start.8 = (f32[2048]{0:T(1024)S(1)}, f32[2048]{0:T(1024)}, u32[]{:S(2)}) copy-start(f32[2048]{0:T(1024)} %param.25) | copy-start | bytes 24580
  152.0 50.6 %all-to-all-start.1 = ((bf16[8,96,512]{2,1,0:T(8,128)(2,1)}), bf16[8,96,512]{2,1,0:T(8,128)(2,1)S(1)}, u32[]{:S(2)}, u32[]{:S(2)}) async-start(bf16[8,96,512]{2,1,0:T(8,128)(2,1)} %bitcast.137), calls=%async_computation.2 | async-start | bytes 1572864 | tf_op jit(solution)/shard_map/all_to_all | solution.py:179
  199.1 1.9 copy-start.2
  (2 other events, 2.2 us)
Sparse Core Ops, SparseCore 0:
  43.5 30.1 all-gather.1
  99.1 50.7 reduce-scatter.1
  152.9 46.1 all-reduce.1
where the time goes:
time: 219 us; the launch traced here: 216 us
  matrix products  59.3 us (27%)
  blocking collectives  52.3 us (24%)
  waiting for transfers between devices  41.7 us (19%)
  local copies, waits for them, and re-layouts  25.2 us (12%)
  other arithmetic  17.9 us (8%)
  between operations  14.2 us (6%)
  starting transfers between devices  5.56 us (3%)
    psum x1, waiting for transfers between devices, mixer_half(): lax.psum(partial_value.astype(jnp.bfloat16), 'tp').astype(jnp.float32)  41.4 us
    all_gather x1, blocking collectives, mixer_half(): piece = lax.all_gather(stacked, 'ep', axis=0, tiled=True)  29 us
    all_to_all x1, blocking collectives, expert_half(): lax.all_to_all(outgoing, 'ep', split_axis=0, concat_axis=0, tiled=True)  23.3 us
    dot_general x8, matrix products, step_block(): jnp.einsum('kgqs,skd->kgqd', exponent.astype(jnp.bfloat16), block_values,...  20 us
    dot_general x8, matrix products, step_block(): jnp.einsum('qkgd,skd->kgqs', query_grouped, block_keys, preferred_element...  15.3 us
    dynamic_slice x16, local copies, waits for them, and re-layouts, mixer_half(): carry, unused = lax.scan(step_block, carry, blocks)  8.23 us
    dot_general x1, matrix products, expert_half(): jnp.einsum('esd,edf->esf', piece, gate_weight, preferred_element_type=jnp...  6.28 us
    all_to_all x1, starting transfers between devices, expert_half(): lax.all_to_all(routed_slots, 'ep', split_axis=0, concat_axis=0, tiled=True)  5.44 us
  transfers between devices with their start and end apart: 4, of which 2 were waited for; matrix products, arithmetic and copies ran while one was open for 30% of the time, Pallas kernels for 0%

commit v1 on v0

v1 whole, which is shorter than its diff:
```python
import functools

import jax
import jax.numpy as jnp
from jax import lax
from jax.experimental import pallas as pl
from jax.experimental.pallas import tpu as pltpu
from jax.sharding import PartitionSpec as P

HEADS = 16
KV_HEADS = 4
HEAD_DIM = 64
GRID_W = 64

EPSILON = 1e-06
ROUTED_SCALE = 2.5
F32 = jnp.float32
BF16 = jnp.bfloat16
MESH = pl.DeviceIdType.MESH


def rotary_angles(position):
    grid_row = (position // GRID_W).astype(F32)
    grid_col = (position % GRID_W).astype(F32)
    quarter = HEAD_DIM // 4
    inverse = 10000.0 ** (-jnp.arange(quarter, dtype=F32) / quarter)
    return jnp.concatenate([grid_row[:, None] * inverse, grid_col[:, None] * inverse], axis=1)


def normalize_rotate(heads_in, gain_vector, angles):
    widened = heads_in.astype(F32)
    scaled = widened * lax.rsqrt(jnp.mean(widened * widened, axis=-1, keepdims=True) + EPSILON)
    scaled = scaled * gain_vector
    half_dim = scaled.shape[-1] // 2
    front_half = scaled[..., :half_dim]
    back_half = scaled[..., half_dim:]
    cosine_table = jnp.cos(angles)[:, None, :]
    sine_table = jnp.sin(angles)[:, None, :]
    turned = jnp.concatenate(
        [
            front_half * cosine_table - back_half * sine_table,
            front_half * sine_table + back_half * cosine_table,
        ],
        axis=-1,
    )
    return turned.astype(BF16)


def silu(v):
    return v / (1.0 + jnp.exp(-v))


def dot(a, b):
    return jnp.dot(a, b, preferred_element_type=F32)


def fused_kernel(
    sizes,
    kv_in, out_in, q_in, normed_in, pick_in, gain_in,
    sg_hbm, su_hbm, sd_hbm, ow_hbm, wg_hbm, wu_hbm, wd_hbm,
    mixer_ref, expert_ref,
    sg, su, sd, ow, wg, wu, wd,
    kv, att, mp, mrecv, msum, my, mo, xh, hid, po, rp, tt, ret,
    sho, shs, shr, cf, cb, cr,
    w_sem, kv_s, kv_r, d_s, d_r, f_s, f_r, sh_sem, mp_sem, my_s, my_r, mo_sem,
    p_s, p_r, r_s, r_r, c_s, c_r,
):
    n, tp_n, ny, heads, cp, lc = sizes
    me = lax.axis_index("ep")
    tp = lax.axis_index("tp")
    core = tp % 2
    y = tp // 2
    mate = tp + 1 - 2 * core
    other = 1 - core
    ra = kv_in.shape[0]
    half = ra // 2

    def send(src, dst, ssem, rsem, ep=None, t=None):
        return pltpu.make_async_remote_copy(
            src_ref=src, dst_ref=dst, send_sem=ssem, recv_sem=rsem,
            device_id=(me if ep is None else ep, tp if t is None else t), device_id_type=MESH,
        )

    def rows(block, size):
        return pl.ds(pl.multiple_of(block * size, size), size)

    def each(lo, hi, fn):
        def step(i, c):
            fn(i)
            return c
        lax.fori_loop(lo, hi, step, 0)

    weights = [
        pltpu.make_async_copy(a, b, w_sem.at[i])
        for i, (a, b) in enumerate(
            ((sg_hbm, sg), (su_hbm, su), (sd_hbm, sd), (ow_hbm, ow), (wg_hbm, wg), (wu_hbm, wu), (wd_hbm, wd))
        )
    ]
    for copy in weights:
        copy.start()

    barrier = pltpu.get_barrier_semaphore()

    def greet(s):
        pl.semaphore_signal(barrier, inc=1, device_id=((me + s) % n, tp), device_id_type=MESH)

    def greet_y(s):
        pl.semaphore_signal(barrier, inc=1, device_id=(me, (tp + 2 * s) % tp_n), device_id_type=MESH)

    each(1, n, greet)
    each(1, ny, greet_y)
    pl.semaphore_signal(barrier, inc=1, device_id=(me, mate), device_id_type=MESH)
    pl.semaphore_wait(barrier, n - 1 + ny - 1 + 1)

    def kv_copy(src, to):
        return send(kv_in, kv.at[rows(src, ra)], kv_s.at[to], kv_r.at[src], ep=to)

    def d_copy(src, to):
        return send(out_in.at[rows(to, cp)], xh.at[core, rows(src, cp)], d_s.at[to], d_r.at[src], ep=to)

    each(1, n, lambda s: kv_copy(me, (me + s) % n).start())
    each(1, n, lambda s: d_copy(me, (me + s) % n).start())

    def own_forward():
        return send(out_in.at[rows(me, cp)], xh.at[core, rows(me, cp)], f_s.at[me], f_r.at[me], t=mate)

    def forward(src):
        return send(xh.at[core, rows(src, cp)], xh.at[core, rows(src, cp)], f_s.at[src], f_r.at[src], t=mate)

    own_forward().start()
    kv[rows(me, ra), :] = kv_in[...]
    xh[core, rows(me, cp), :] = out_in[rows(me, cp), :]

    for i in range(3):
        weights[i].wait()
    normed = normed_in[...]
    sh_hidden = (silu(dot(normed, sg[...])) * dot(normed, su[...])).astype(BF16)

    def cols(tile):
        return pl.ds(pl.multiple_of(tile * lc, lc), lc)

    for q in range(ny):
        sho[q] = dot(sh_hidden, sd[:, cols(2 * q + other)]).astype(BF16)
    sh_copy = send(sho, shr, sh_sem.at[0], sh_sem.at[1], t=mate)
    sh_copy.start()
    for q in range(ny):
        shs[q] = dot(sh_hidden, sd[:, cols(2 * q + core)]).astype(BF16)

    each(1, n, lambda s: kv_copy((me + n - s) % n, me).wait_recv())
    total = kv.shape[0]
    bq = max(16, min(ra, 128 * 3072 // total // 16 * 16))
    while ra % bq:
        bq -= 16
    per_head = ra // bq

    def attend(i):
        block = q_in[pl.ds(pl.multiple_of(i * bq, bq), bq), :]
        scores = lax.dot_general(block, kv[...], (((1,), (1,)), ((), ())), preferred_element_type=F32)
        peak = jnp.max(scores, axis=1, keepdims=True)
        exponent = jnp.exp(scores - peak)
        row_total = jnp.sum(exponent, axis=1, keepdims=True)
        weighted = dot(exponent.astype(BF16), kv[...])
        att[pl.ds(pl.multiple_of((i % per_head) * bq, bq), bq),
            pl.ds(pl.multiple_of((i // per_head) * 128, 128), 128)] = (weighted / row_total).astype(BF16)

    steps = heads * per_head
    pair = 2 if steps % 2 == 0 else 1

    def attend_pair(i):
        for j in range(pair):
            attend(i * pair + j)

    each(0, steps // pair, attend_pair)

    def pass_on(s):
        src = (me + n - s) % n
        d_copy(src, me).wait_recv()
        forward(src).start()

    each(1, n, pass_on)

    weights[3].wait()
    width = mp.shape[1]
    tile = min(512, width)

    def project(t):
        at = pl.ds(pl.multiple_of(t * tile, tile), tile)
        mp[:, at] = dot(att[...], ow[:, at]).astype(BF16)

    each(0, width // tile, project)
    mp_copy = send(mp.at[rows(other, half)], mrecv, mp_sem.at[0], mp_sem.at[1], t=mate)
    mp_copy.start()

    weights[4].wait()
    weights[5].wait()
    each(0, n, lambda s: send(
        xh.at[other, rows(s, cp)], xh.at[other, rows(s, cp)], f_s.at[s], f_r.at[s], t=mate).wait_recv())
    depth = xh.shape[2]
    ft = min(256, hid.shape[1])

    def gate_up(t):
        at = pl.ds(pl.multiple_of(t * ft, ft), ft)
        gate = dot(xh[0], wg[0:depth, at]) + dot(xh[1], wg[depth:, at])
        up = dot(xh[0], wu[0:depth, at]) + dot(xh[1], wu[depth:, at])
        hid[:, at] = (silu(gate) * up).astype(BF16)

    each(0, 1, gate_up)
    mp_copy.wait_recv()
    msum[...] = (mp[rows(core, half), :].astype(F32) + mrecv[...].astype(F32)).astype(BF16)

    def my_copy(src, to):
        return send(msum, my.at[src], my_s.at[to], my_r.at[src], t=2 * to + core)

    each(1, ny, lambda s: my_copy(y, (y + s) % ny).start())
    my[y] = msum[...]
    each(1, hid.shape[1] // ft, gate_up)

    weights[6].wait()

    def p_copy(q):
        return send(po.at[q], rp.at[q], p_s.at[q], p_r.at[q], t=mate)

    def down_other(q):
        po[q] = dot(hid[...], wd[:, cols(2 * q + other)]).astype(BF16)
        p_copy(q).start()

    each(0, ny, down_other)

    def r_copy(q, src, to):
        return send(tt.at[q, rows(to, cp)], ret.at[q, rows(src, cp)], r_s.at[q, to], r_r.at[q, src], ep=to)

    def down_own(q):
        own = dot(hid[...], wd[:, cols(2 * q + core)]).astype(BF16).astype(F32)
        p_copy(q).wait_recv()
        tt[q] = (own + rp[q].astype(F32)).astype(BF16)
        each(1, n, lambda s: r_copy(q, me, (me + s) % n).start())
        ret[q, rows(me, cp), :] = tt[q, rows(me, cp), :]

    def down_step(s):
        down_own((y + s) % ny)

    each(1, ny + 1, down_step)

    each(1, ny, lambda s: my_copy((y + s) % ny, y).wait_recv())
    mixed = my[0].astype(F32)
    for j in range(1, ny):
        mixed = mixed + my[j].astype(F32)
    scale = lax.rsqrt(jnp.mean(mixed * mixed, axis=1, keepdims=True) + EPSILON)
    msum_out = (mixed * scale * gain_in[...]).astype(BF16)
    mixer_ref[rows(core, half), :] = msum_out
    mp_copy.wait_send()
    mp[rows(core, half), :] = msum_out
    mo_copy = send(mp.at[rows(core, half)], mo, mo_sem.at[0], mo_sem.at[1], t=mate)
    mo_copy.start()
    mo_copy.wait_recv()
    mixer_ref[rows(other, half), :] = mo[...]

    sh_copy.wait_recv()

    def combine(q):
        each(1, n, lambda s: r_copy(q, (me + n - s) % n, me).wait_recv())
        routed = dot(pick_in[0], ret[q]) + dot(pick_in[1], ret[q])
        return routed + shs[q].astype(F32) + shr[q].astype(F32)

    def c_copy(src, to):
        return send(cb.at[to], cr.at[src], c_s.at[to], c_r.at[src], t=2 * to + core)

    def combine_far(s):
        q = (y + s) % ny
        cb[q] = combine(q).astype(BF16)
        c_copy(y, q).start()

    each(1, ny, combine_far)
    cf[...] = combine(y)

    def collect(s):
        src = (y + s) % ny
        c_copy(src, y).wait_recv()
        cf[...] += cr[src].astype(F32)

    each(1, ny, collect)
    expert_ref[...] = cf[...].astype(BF16)

    def drain(s):
        to = (me + s) % n
        kv_copy(me, to).wait_send()
        d_copy(me, to).wait_send()
        forward((me + s) % n).wait_send()
        each(0, ny, lambda q: r_copy(q, me, to).wait_send())

    each(1, n, drain)
    own_forward().wait_send()
    sh_copy.wait_send()
    mo_copy.wait_send()
    each(0, ny, lambda q: p_copy(q).wait_send())

    def drain_y(s):
        to = (y + s) % ny
        my_copy(y, to).wait_send()
        c_copy(y, to).wait_send()

    each(1, ny, drain_y)


def body(
    query_rows, key_rows, value_rows, query_gain, key_gain, out_weight, mixer_gain,
    expert_input, expert_ids, gate_score, expert_gain,
    gate_weight, up_weight, down_weight, shared_gate, shared_up, shared_down,
):
    n = lax.axis_size("ep")
    tp_n = lax.axis_size("tp")
    ny = tp_n // 2
    me = lax.axis_index("ep")
    tp = lax.axis_index("tp")
    ra = query_rows.shape[0]
    heads = query_rows.shape[1] // HEAD_DIM
    first_kv = tp * heads // (HEADS // KV_HEADS)
    angles = rotary_angles(me * ra + jnp.arange(ra, dtype=jnp.int32))
    query_rot = normalize_rotate(query_rows.reshape(ra, heads, HEAD_DIM), query_gain, angles)
    query_rot = query_rot * BF16(HEAD_DIM ** (-0.5))
    q_in = jnp.pad(query_rot.transpose(1, 0, 2), ((0, 0), (0, 0), (0, HEAD_DIM))).reshape(heads * ra, 2 * HEAD_DIM)
    key_cols = lax.dynamic_slice_in_dim(key_rows, first_kv * HEAD_DIM, HEAD_DIM, 1)
    value_cols = lax.dynamic_slice_in_dim(value_rows, first_kv * HEAD_DIM, HEAD_DIM, 1)
    key_rot = normalize_rotate(key_cols.reshape(ra, 1, HEAD_DIM), key_gain, angles)
    kv_in = jnp.concatenate([key_rot.reshape(ra, HEAD_DIM), value_cols], axis=1)
    width = out_weight.shape[1]
    ow_pad = jnp.pad(out_weight.reshape(heads, HEAD_DIM, width), ((0, 0), (HEAD_DIM, 0), (0, 0)))
    ow_pad = ow_pad.reshape(heads * 2 * HEAD_DIM, width)
    rb, top = expert_ids.shape
    experts = n * gate_weight.shape[0]
    cap = 3 * rb * top // (2 * experts)
    cp = -(-cap // 16) * 16
    model = expert_input.shape[1]
    lc = model // tp_n
    widened = expert_input.astype(F32)
    normed = (
        widened * lax.rsqrt(jnp.mean(widened * widened, axis=1, keepdims=True) + EPSILON) * expert_gain
    ).astype(BF16)
    route_weight = gate_score / jnp.sum(gate_score, axis=1, keepdims=True) * ROUTED_SCALE
    named = expert_ids[:, :, None] == jnp.arange(experts, dtype=jnp.int32)
    member = jnp.any(named, axis=1)
    row_weight = jnp.sum(jnp.where(named, route_weight[:, :, None], 0.0), axis=1)
    before = jnp.tril(jnp.ones((rb, rb), BF16), -1)
    rank = dot(before, member.astype(BF16)).astype(jnp.int32)
    slot = jnp.where(member, rank, -1)
    chosen = slot[:, :, None] == jnp.arange(cp, dtype=jnp.int32)
    weight = jnp.where(chosen, row_weight[:, :, None], 0.0).reshape(rb, experts * cp)
    high = weight.astype(BF16)
    low = (weight - high.astype(F32)).astype(BF16)
    pick = jnp.stack([high, low])
    choose = chosen.astype(BF16).reshape(rb, experts * cp)
    own_cols = lax.dynamic_slice_in_dim(normed, (tp % 2) * (model // 2), model // 2, 1)
    outgoing = lax.dot_general(
        choose, own_cols, (((0,), (0,)), ((), ())), preferred_element_type=F32
    ).astype(BF16)

    slots = n * cp
    hidden = gate_weight.shape[2]
    sh = shared_gate.shape[1]
    vm = pltpu.VMEM
    dma = pltpu.SemaphoreType.DMA
    half = ra // 2
    vspec = pl.BlockSpec(memory_space=pltpu.VMEM)
    hspec = pl.BlockSpec(memory_space=pl.ANY)
    sizes = (n, tp_n, ny, heads, cp, lc)
    return pl.pallas_call(
        functools.partial(fused_kernel, sizes),
        out_shape=(
            jax.ShapeDtypeStruct((ra, width), BF16),
            jax.ShapeDtypeStruct((rb, lc), BF16),
        ),
        in_specs=[vspec] * 6 + [hspec] * 7,
        out_specs=(vspec, vspec),
        scratch_shapes=[
            vm((model, sh), BF16), vm((model, sh), BF16), vm((sh, model), BF16),
            vm((heads * 2 * HEAD_DIM, width), BF16),
            vm((model, hidden), BF16), vm((model, hidden), BF16), vm((hidden, model), BF16),
            vm((n * ra, 2 * HEAD_DIM), BF16),
            vm((ra, heads * 2 * HEAD_DIM), BF16),
            vm((ra, width), BF16), vm((half, width), BF16), vm((half, width), BF16),
            vm((ny, half, width), BF16), vm((half, width), BF16),
            vm((2, slots, model // 2), BF16), vm((slots, hidden), BF16),
            vm((ny, slots, lc), BF16), vm((ny, slots, lc), BF16),
            vm((ny, slots, lc), BF16), vm((ny, slots, lc), BF16),
            vm((ny, rb, lc), BF16), vm((ny, rb, lc), BF16), vm((ny, rb, lc), BF16),
            vm((rb, lc), F32), vm((ny, rb, lc), BF16), vm((ny, rb, lc), BF16),
            dma((7,)), dma((n,)), dma((n,)), dma((n,)), dma((n,)), dma((n,)), dma((n,)),
            dma((2,)), dma((2,)), dma((ny,)), dma((ny,)), dma((2,)),
            dma((ny,)), dma((ny,)), dma((ny, n)), dma((ny, n)), dma((ny,)), dma((ny,)),
        ],
        compiler_params=pltpu.CompilerParams(
            collective_id=0, has_side_effects=True, vmem_limit_bytes=64 * 1024 * 1000
        ),
        name="fused_layer",
    )(
        kv_in, outgoing, q_in, normed, pick, mixer_gain.reshape(1, width),
        shared_gate, shared_up, shared_down, ow_pad,
        gate_weight[0], up_weight[0], down_weight[0],
    )


def solution(mesh):
    in_specs = (
        P("ep", "tp"), P("ep", None), P("ep", None), P(), P(), P("tp", None), P(),
        P("ep", None), P("ep", None), P("ep", None), P(),
        P("ep", None, "tp"), P("ep", None, "tp"), P("ep", "tp", None),
        P(None, "tp"), P(None, "tp"), P("tp", None),
    )
    out_specs = (P("ep", None), P("ep", "tp"))
    return jax.shard_map(body, mesh=mesh, in_specs=in_specs, out_specs=out_specs, check_vma=False)
```

time: 219 us -> 127 us (0.58); the launches traced: 216 us -> 127 us
  Pallas kernels: 0 us -> 107 us
  matrix products: 59.3 us -> 1.96 us
  blocking collectives: 52.3 us -> 0 us
  waiting for transfers between devices: 41.7 us -> 0 us
  local copies, waits for them, and re-layouts: 25.2 us -> 7.84 us
  between operations: 14.2 us -> 0.96 us
  other arithmetic: 17.9 us -> 9.5 us
  starting transfers between devices: 5.56 us -> 0 us
    pallas_call x0 -> x1, Pallas kernels: none -> 107 us  [body(): pl.pallas_call(functools.partial(fused_kernel, sizes), out_shape=(jax.Sha...]
    dot_general x22 -> x2, matrix products: 59.3 us -> 1.96 us  [the longest x1 1.73 us: body(): lax.dot_general(choose, own_cols, (((0,), (0,)), ((), ())), preferred_ele...]
    psum x1 -> x0, waiting for transfers between devices: 41.4 us -> none  [mixer_half(): lax.psum(partial_value.astype(jnp.bfloat16), 'tp').astype(jnp.float32)]
    all_gather x1 -> x0, blocking collectives: 29 us -> none  [mixer_half(): piece = lax.all_gather(stacked, 'ep', axis=0, tiled=True)]
    all_to_all x1 -> x0, blocking collectives: 23.3 us -> none  [expert_half(): lax.all_to_all(outgoing, 'ep', split_axis=0, concat_axis=0, tiled=True)]
    dynamic_slice x18 -> x1, local copies, waits for them, and re-layouts: 9.31 us -> 0.1 us  [body(): lax.dynamic_slice_in_dim(value_rows, first_kv * HEAD_DIM, HEAD_DIM, 1)]
    all_to_all x1 -> x0, starting transfers between devices: 5.44 us -> none  [expert_half(): lax.all_to_all(routed_slots, 'ep', split_axis=0, concat_axis=0, tiled=True)]
    gather x2 -> x0, local copies, waits for them, and re-layouts: 5.3 us -> none  [the longest x1 2.68 us: expert_half(): own_cols[safe_rows]]
  transfers between devices with their start and end apart: 4 -> 0, of which waited for: 2 -> 0; matrix products, arithmetic and copies ran while one was open for 30% -> 0% of each run, Pallas kernels for 0% -> 0%
where the time goes in v1:
time: 127 us
  Pallas kernels  107 us (84%)
  other arithmetic  9.5 us (7%)
  local copies, waits for them, and re-layouts  7.84 us (6%)
  matrix products  1.96 us (2%)
    pallas_call x1, Pallas kernels, body(): pl.pallas_call(functools.partial(fused_kernel, sizes), out_shape=(jax.Sha...  107 us
    unnamed x24, local copies, waits for them, and re-layouts  4.34 us

profile of v1, /device:TPU:27, one launch (start us, length us, event | category | flops | bytes accessed | tf_op | source)
XLA Modules:
  0.0 126.9 jit_solution(4137588741116508048)
XLA Ops:
  0.7 1.6 %fusion = f32[256]{0:T(256)S(1)} fusion(bf16[256,2048]{1,0:T(8,128)(2,1)} %param.24), kind=kLoop, calls=%fused_computation.2 | loop fusion | flops 1572608 | bytes 1049600 | tf_op jit(solution)/shard_map/reduce_sum | solution.py:337
  2.3 0.7 reduce_sum.48
  3.1 0.7 divide_multiply_fusion
  3.7 1.1 fusion.9
  4.9 0.7 fusion.21
  5.7 0.2 fusion.3
  5.9 0.7 select_reduce_fusion
  6.7 0.2 fusion.20
  7.0 0.2 pad_maximum_fusion.2
  7.9 0.2 copy.52
  8.2 0.9 pad.8.clone
  9.2 0.7 fusion.15
  9.9 0.8 pad_maximum_fusion.1.kv_in
  10.6 0.2 bitcast_compare_fusion
  10.9 0.3 copy.50
  11.2 0.3 copy.51
  11.7 1.0 pad_maximum_fusion.pick_in
  12.7 0.4 copy-done.2
  13.1 0.3 fusion.2.normed_in
  13.4 1.7 %convolution_convert_fusion.out_in = bf16[768,1024]{1,0:T(8,128)(2,1)} fusion(pred[256,768]{0,1:T(32,128)(4,1)S(1)} %bitcast_compare_fusion, bf16[256,2048]{1,0:T(8,128)(2,1)S(1)} %fusion.2.normed_in, s32[]{:T(128)S(6)} %select_n.72), kind=kOutput, calls=%fused_computation.5 | convolution fusion | flops 403439616 | bytes 2293764 | tf_op jit(solution)/shard_map/dot_general | solution.py:353
  15.2 1.6 %pad.9 = bf16[4,128,2048]{2,1,0:T(8,128)(2,1)} pad(bf16[4,64,2048]{2,1,0:T(8,128)(2,1)S(1)} %bitcast.36, bf16[]{:T(256)} %constant.98.clone.1), padding=0_0x64_0x0_0 | pad | bytes 3145730 | tf_op jit(solution)/shard_map/jit(_pad)/pad | solution.py:327
  16.8 106.6 %fused_layer.1 = (bf16[384,2048]{1,0:T(8,128)(2,1)}, bf16[256,512]{1,0:T(8,128)(2,1)}) custom-call(bf16[384,128]{1,0:T(8,128)(2,1)} %pad_maximum_fusion.1.kv_in, bf16[768,1024]{1,0:T(8,128)(2,1)} %convolution_convert_fusion.out_in, bf16[1536,128]{1,0:T(8,128)(2,1)} %bitcast.35, bf16[256,2048]{1,0:T(8,128)(2,1)} %copy-done.1, ...), custom_call_target="tpu_custom_call" | custom-call | tf_op jit(solution)/shard_map/fused_layer/pallas_call | solution.py:366
  123.4 2.8 %copy.57 = bf16[384,2048]{1,0:T(8,128)(2,1)} copy(bf16[384,2048]{1,0:T(8,128)(2,1)} %get-tuple-element.20) | data formatting | bytes 3145728
  126.2 0.7 copy.58
  (41 shorter events, 1.5 us)
Async XLA Ops:
  0.6 6.2 %copy-start = (bf16[384,256]{1,0:T(8,128)(2,1)S(1)}, bf16[384,256]{1,0:T(8,128)(2,1)}, u32[]{:S(2)}) copy-start(bf16[384,256]{1,0:T(8,128)(2,1)} %param.19) | copy-start | bytes 589828
  0.6 6.7 %copy-start.6 = (bf16[384,256]{1,0:T(8,128)(2,1)S(1)}, bf16[384,256]{1,0:T(8,128)(2,1)}, u32[]{:S(2)}) copy-start(bf16[384,256]{1,0:T(8,128)(2,1)} %param.18) | copy-start | bytes 589828
  0.7 6.7 %copy-start.8 = (f32[64]{0:T(128)S(1)}, f32[64]{0:T(128)}, u32[]{:S(2)}) copy-start(f32[64]{0:T(128)} %param.21) | copy-start | bytes 772
  0.7 7.1 %copy-start.9 = (f32[64]{0:T(128)S(1)}, f32[64]{0:T(128)}, u32[]{:S(2)}) copy-start(f32[64]{0:T(128)} %param.20) | copy-start | bytes 772
  0.7 6.8 %copy-start.5 = (bf16[384,256]{1,0:T(8,128)(2,1)S(1)}, bf16[384,256]{1,0:T(8,128)(2,1)}, u32[]{:S(2)}) copy-start(bf16[384,256]{1,0:T(8,128)(2,1)} %param.17) | copy-start | bytes 589828
  11.6 1.5 %copy-start.2 = (bf16[256,2048]{1,0:T(8,128)(2,1)S(1)}, bf16[256,2048]{1,0:T(8,128)(2,1)}, u32[]{:S(2)}) copy-start(bf16[256,2048]{1,0:T(8,128)(2,1)} %param.24) | copy-start | bytes 3145732
  11.6 1.5 %copy-start.7 = (f32[2048]{0:T(1024)S(1)}, f32[2048]{0:T(1024)}, u32[]{:S(2)}) copy-start(f32[2048]{0:T(1024)} %param.27) | copy-start | bytes 24580
  13.1 2.1 %copy-start.3 = (bf16[256,2048]{1,0:T(8,128)(2,1)S(1)}, bf16[256,2048]{1,0:T(8,128)(2,1)}, u32[]{:S(2)}) copy-start(bf16[256,2048]{1,0:T(8,128)(2,1)} %param.22) | copy-start | bytes 3145732
  13.4 3.3 %copy-start.1 = (bf16[256,2048]{1,0:T(8,128)(2,1)}, bf16[256,2048]{1,0:T(8,128)(2,1)S(1)}, u32[]{:S(2)}) copy-start(bf16[256,2048]{1,0:T(8,128)(2,1)S(1)} %fusion.2.normed_in) | copy-start | bytes 3145732
  123.4 2.8 %copy-start.4 = (bf16[256,512]{1,0:T(8,128)(2,1)S(1)}, bf16[256,512]{1,0:T(8,128)(2,1)}, u32[]{:S(2)}) copy-start(bf16[256,512]{1,0:T(8,128)(2,1)} %get-tuple-element.21) | copy-start | bytes 786436
